TPU v7x, 512 devices: a whole 4x8x8 slice. The times are simulated.
512 devices in a mesh: ep: 32 (over z, x), tp: 16 (over y, core).
Axes of the slice: x: 4, y: 8, z: 8, core: 2. Of those that a mesh axis runs over, the one named last changes fastest.
Arguments:
- queries: bfloat16 [8192, 2048], P('ep', 'tp'), may hold values from -9 to 9
- key_rows: bfloat16 [8192, 2048], P('ep', 'tp'), may hold values from -9 to 9
- values: bfloat16 [8192, 2048], P('ep', 'tp'), may hold values from -6 to 6
- second_scale: float32 [16], P('tp'), may hold values from 0.3 to 0.8
- head_gain: float32 [128], replicated, may hold values from 0.1 to 1.9
- out_weight: bfloat16 [2048, 2048], P(None, 'tp'), may hold values from -0.125 to 0.125
- routed_in: bfloat16 [8192, 2048], P('ep'), may hold values from -6 to 6
- routed_gain: float32 [2048], replicated, may hold values from 0.1 to 1.9
- expert_ids: int32 [8192, 2], P('ep'), may hold values from 0 to 31, all different within a row; in each aligned block of 256 rows (0 to 255, 256 to 511, ...) at most 32 rows name the same one
- group_logits: float32 [8192, 8], P('ep'), may hold values from -6 to 6
- inner_logits: float32 [8192, 2], P('ep'), may hold values from -6 to 6
- gate_weight: bfloat16 [32, 2048, 4096], P('ep', None, 'tp'), may hold values from -0.125 to 0.125
- up_weight: bfloat16 [32, 2048, 4096], P('ep', None, 'tp'), may hold values from -0.125 to 0.125
- down_weight: bfloat16 [32, 4096, 2048], P('ep', 'tp'), may hold values from -0.09375 to 0.09375
Outputs:
- mixer_out: bfloat16 [8192, 2048], P('ep', 'tp')
- routed_out: bfloat16 [8192, 2048], P('ep', 'tp')
Inputs may be any that keep to these rules, and one draw needn't show every extreme that they name: `expert_ids`: the two ids of a row differ. In the rows of one device (aligned blocks of 256 rows) no expert is named by more than 32 rows, a bound that some block reaches.
All inputs are finite; a program needn't handle non-finite values.
Results may differ from a plain program's by a relative error of at most 0.018.
Values may be sent and summed in bfloat16 or wider, within the bound.
A program may use at most 128 MiB of HBM per device.

v0:
```python
import math
import jax
import jax.numpy as jnp
from jax import lax
from jax.sharding import Mesh
from jax.sharding import PartitionSpec as P

GROUP_SIZE = 4
EP = ("ep_0", "ep_1")
EPSILON = 1e-05
LOWEST = -1e30


def whole_of(array, axes, dim):
    if not axes:
        return array
    nearer = lax.all_gather(array, axes[-1], axis=dim, tiled=True)
    return whole_of(nearer, axes[:-1], dim)


def token_mixer(queries, key_rows, values, second_scale, head_gain, out_weight):
    row_count = queries.shape[0]
    local_heads = second_scale.shape[0]
    qk_size = queries.shape[1] // (2 * local_heads)
    value_size = values.shape[1] // local_heads
    first_pos = lax.axis_index(EP) * row_count
    query_pos = first_pos + jnp.arange(row_count, dtype=jnp.int32)
    last_pos = first_pos + row_count - 1
    query_four = queries.reshape(row_count, local_heads, 2, qk_size)
    score_scale = qk_size ** (-0.5)
    initial = (
        jnp.full((row_count, local_heads, 2), LOWEST, jnp.float32),
        jnp.zeros((row_count, local_heads, 2), jnp.float32),
        jnp.zeros((row_count, local_heads, 2, value_size), jnp.float32),
    )
    state_now = initial
    key_piece = whole_of(key_rows, EP, 0)
    value_piece = whole_of(values, EP, 0)
    piece_count = key_piece.shape[0]
    block_width = math.gcd(piece_count, 512)
    blocks = piece_count // block_width
    key_blocks = key_piece.reshape(blocks, block_width, local_heads, 2, qk_size)
    value_blocks = value_piece.reshape(blocks, block_width, local_heads, value_size)

    def update(state_inner, block_index):
        key_start = block_index * block_width

        def attend(inner_state):
            running_max, denominator, weighted = inner_state
            scores = (
                jnp.einsum(
                    "qhmd,khmd->qhmk",
                    query_four,
                    key_blocks[block_index],
                    preferred_element_type=jnp.float32,
                )
                * score_scale
            )
            key_pos = key_start + jnp.arange(block_width, dtype=jnp.int32)
            visible = (query_pos[:, None] >= key_pos[None, :])[:, None, None, :]
            scores = jnp.where(visible, scores, LOWEST)
            new_max = jnp.maximum(running_max, jnp.max(scores, axis=-1))
            exp_terms = jnp.where(visible, jnp.exp(scores - new_max[..., None]), 0.0)
            factor = jnp.exp(running_max - new_max)
            denominator = denominator * factor + jnp.sum(exp_terms, axis=-1)
            weighted = weighted * factor[..., None] + jnp.einsum(
                "qhmk,khe->qhme",
                exp_terms.astype(jnp.bfloat16),
                value_blocks[block_index],
                preferred_element_type=jnp.float32,
            )
            return (new_max, denominator, weighted)

        return (
            lax.cond(key_start <= last_pos, attend, lambda inner_state: inner_state, state_inner),
            None,
        )

    state_now, _ = lax.scan(update, state_now, jnp.arange(blocks, dtype=jnp.int32))
    running_max, denominator, weighted = state_now
    mapped = weighted / denominator[..., None]
    difference = mapped[:, :, 0] - second_scale[None, :, None] * mapped[:, :, 1]
    inv_norm = lax.rsqrt(jnp.mean(difference * difference, axis=-1, keepdims=True) + EPSILON)
    head_out = (
        (difference * inv_norm * head_gain)
        .astype(jnp.bfloat16)
        .reshape(row_count, local_heads * value_size)
    )
    mixed = jnp.dot(
        lax.all_gather(head_out, "tp", axis=1, tiled=True),
        out_weight,
        preferred_element_type=jnp.float32,
    )
    return mixed.astype(jnp.bfloat16)


def expert_block(
    routed_in,
    routed_gain,
    expert_ids,
    group_logits,
    inner_logits,
    gate_weight,
    up_weight,
    down_weight,
):
    token_count = routed_in.shape[0]
    chosen = expert_ids.shape[1]
    ep_size = lax.axis_size(EP)
    capacity = 2 * chosen * token_count // ep_size
    source = routed_in.astype(jnp.float32)
    normed = (
        source
        * lax.rsqrt(jnp.mean(source * source, axis=-1, keepdims=True) + EPSILON)
        * routed_gain
    ).astype(jnp.bfloat16)
    flat_ids = expert_ids.reshape(-1)
    picked = (flat_ids[:, None] == jnp.arange(ep_size, dtype=jnp.int32)[None, :]).astype(jnp.int32)
    slot_index = jnp.sum(jnp.cumsum(picked, axis=0) * picked, axis=1) - 1
    place_index = flat_ids * capacity + slot_index
    owner_row = jnp.arange(token_count * chosen, dtype=jnp.int32) // chosen
    slot_rows = jnp.zeros((ep_size * capacity,), jnp.int32).at[place_index].set(owner_row)
    outgoing = normed[slot_rows].reshape(ep_size, capacity, normed.shape[1])
    gate_local = gate_weight[0]
    up_local = up_weight[0]
    down_local = down_weight[0]
    columns = outgoing.shape[2] // lax.axis_size("tp")
    own_columns = lax.dynamic_slice_in_dim(outgoing, lax.axis_index("tp") * columns, columns, 2)
    arrived = lax.all_to_all(own_columns, EP, split_axis=0, concat_axis=0, tiled=True)
    experts_arrived = lax.all_gather(arrived, "tp", axis=2, tiled=True)
    stacked = experts_arrived.reshape(-1, experts_arrived.shape[2])
    gate_act = jnp.dot(stacked, gate_local, preferred_element_type=jnp.float32)
    up_act = jnp.dot(stacked, up_local, preferred_element_type=jnp.float32)
    hidden = (jax.nn.silu(gate_act) * up_act).astype(jnp.bfloat16)
    partial_value = jnp.dot(hidden, down_local, preferred_element_type=jnp.float32)
    partial_value = partial_value.reshape(
        experts_arrived.shape[0], experts_arrived.shape[1], partial_value.shape[1]
    )
    answered = lax.psum_scatter(
        partial_value.astype(jnp.bfloat16), "tp", scatter_dimension=2, tiled=True
    )
    returned = lax.all_to_all(answered, EP, split_axis=0, concat_axis=0, tiled=True)
    pair_out = returned.reshape(ep_size * capacity, returned.shape[2])[place_index]
    pair_out = pair_out.reshape(token_count, chosen, returned.shape[2])
    group_prob = jax.nn.softmax(group_logits, axis=-1)
    member = (
        expert_ids[..., None] // GROUP_SIZE == jnp.arange(group_logits.shape[1], dtype=jnp.int32)
    ).astype(jnp.float32)
    group_pick = jnp.sum(group_prob[:, None, :] * member, axis=-1)
    route_weight = group_pick * jax.nn.softmax(inner_logits, axis=-1)
    return jnp.sum(route_weight[..., None] * pair_out.astype(jnp.float32), axis=1).astype(
        jnp.bfloat16
    )


def local(
    queries,
    key_rows,
    values,
    second_scale,
    head_gain,
    out_weight,
    routed_in,
    routed_gain,
    expert_ids,
    group_logits,
    inner_logits,
    gate_weight,
    up_weight,
    down_weight,
):
    mixer_out = token_mixer(queries, key_rows, values, second_scale, head_gain, out_weight)
    routed_out = expert_block(
        routed_in,
        routed_gain,
        expert_ids,
        group_logits,
        inner_logits,
        gate_weight,
        up_weight,
        down_weight,
    )
    return (mixer_out, routed_out)


def solution(mesh):
    finer = Mesh(mesh.devices.reshape(8, 4, mesh.shape["tp"]), ("ep_0", "ep_1", "tp"))
    placed = (
        P(EP, "tp"),
        P(EP, "tp"),
        P(EP, "tp"),
        P("tp"),
        P(),
        P(None, "tp"),
        P(EP, None),
        P(),
        P(EP, None),
        P(EP, None),
        P(EP, None),
        P(EP, None, "tp"),
        P(EP, None, "tp"),
        P(EP, "tp", None),
    )
    return jax.shard_map(
        local, mesh=finer, in_specs=placed, out_specs=(P(EP, "tp"), P(EP, "tp")), check_vma=False
    )
```

profile of v0, /device:TPU:1, one launch (start us, length us, event | category | flops | bytes accessed | tf_op | source)
XLA Modules:
  0.0 325.3 jit_solution(6230517476498490236)
XLA Ops:
  7.2 0.9 copy.52
  8.4 0.7 and_select_fusion
  9.1 1.2 reduce-window.6
  11.0 2.4 scatter_custom_fusion
  13.5 1.5 fusion.21
  15.0 1.5 fusion.23
  16.6 6.0 %gather_fusion = bf16[1024,2048]{1,0:T(8,128)(2,1)} fusion(bf16[256,2048]{1,0:T(8,128)(2,1)S(1)} %fusion.23, s32[1024]{0:T(1024)S(1)} %fusion.38), kind=kCustom, calls=%fused_computation | custom fusion | bytes 8392704 | tf_op jit(solution)/shard_map/gather | solution.py:123
  22.6 1.0 constant_dynamic-slice_fusion
  23.5 24.9 %all_to_all.10 = bf16[32,32,128]{2,1,0:T(8,128)(2,1)} all-to-all(bf16[32,32,128]{2,1,0:T(8,128)(2,1)S(1)} %constant_dynamic-slice_fusion), channel_id=1, replica_groups=mesh['ep_0'=8,'ep_1'=4,'tp'=16] {'ep_0','ep_1'}, dimensions={0} | all-to-all | bytes 524288 | tf_op jit(solution)/shard_map/all_to_all | solution.py:129
  48.6 10.7 %all_gather.18 = bf16[1024,128]{1,0:T(8,128)(2,1)} all-gather(bf16[256,128]{1,0:T(8,128)(2,1)S(1)} %copy-done.3), channel_id=1, replica_groups=mesh['ep_0'=8,'ep_1'=4,'tp'=16] {'ep_1'}, dimensions={0}, use_global_device_ids=true | all-gather | bytes 327680 | tf_op jit(solution)/shard_map/all_gather | solution.py:17
  59.4 11.1 %all_gather.20 = bf16[1024,128]{1,0:T(8,128)(2,1)} all-gather(bf16[256,128]{1,0:T(8,128)(2,1)S(1)} %copy-done.4), channel_id=1, replica_groups=mesh['ep_0'=8,'ep_1'=4,'tp'=16] {'ep_1'}, dimensions={0}, use_global_device_ids=true | all-gather | bytes 327680 | tf_op jit(solution)/shard_map/all_gather | solution.py:17
  70.6 28.3 %all-gather.11.cloned.1.call-done = bf16[32,32,2048]{2,1,0:T(8,128)(2,1)} async-done(((bf16[32,32,128]{2,1,0:T(8,128)(2,1)}), bf16[32,32,2048]{2,1,0:T(8,128)(2,1)}) %all-gather.11.cloned.1.call-update) | async-done | bytes 4194320 | tf_op jit(solution)/shard_map/all_gather | solution.py:130
  98.8 3.6 %fusion.27 = f32[1024,256]{1,0:T(8,128)S(1)} fusion(bf16[1024,2048]{1,0:T(8,128)(2,1)} %bitcast.107, bf16[1,2048,256]{2,1,0:T(8,128)(2,1)S(1)} %copy-done.9), kind=kOutput, calls=%fused_computation.42 | convolution fusion | flops 1073741824 | bytes 6291456 | tf_op jit(solution)/shard_map/dot_general | solution.py:132
  102.4 1.3 fusion.24
  103.7 3.2 convolution_convert_fusion
  106.9 23.0 %copy.58 = bf16[32,32,2048]{1,0,2:T(8,128)(2,1)} copy(bf16[32,32,2048]{2,1,0:T(8,128)(2,1)} %convolution_convert_fusion) | data formatting | bytes 8388608
  130.0 23.3 %reshape.280 = bf16[2048,1024]{1,0:T(8,128)(2,1)} reshape(bf16[2048,32,32]{2,1,0:T(8,128)(2,1)} %bitcast.93) | data formatting | bytes 8388608
  154.9 8.2 %reshape.279 = bf16[16,512,1,2,64]{4,3,1,0,2:T(2,128)(2,1)} reshape(bf16[8192,128]{1,0:T(8,128)(2,1)} %all-gather.5.cloned.1.call-done) | data formatting | bytes 4194304 | tf_op jit(solution)/shard_map/reshape | solution.py:42
  163.1 9.1 %copy.48 = bf16[16,512,1,2,64]{1,4,3,2,0:T(8,128)(2,1)S(1)} copy(bf16[16,512,1,2,64]{4,3,1,0,2:T(2,128)(2,1)} %reshape.279) | data formatting | bytes 4194304
  172.2 10.3 %all-gather.7.cloned.1.call-done = bf16[8192,128]{1,0:T(8,128)(2,1)} async-done(((bf16[1024,128]{1,0:T(8,128)(2,1)}), bf16[8192,128]{1,0:T(8,128)(2,1)}) %all-gather.7.cloned.1.call-update) | async-done | bytes 2097168 | tf_op jit(solution)/shard_map/all_gather | solution.py:17
  182.6 3.9 %copy.49 = bf16[16,512,1,128]{1,3,2,0:T(8,128)(2,1)} copy(bf16[16,512,1,128]{3,1,0,2:T(8,128)(2,1)} %bitcast.98) | data formatting | bytes 4194304
  186.6 24.3 %while.15 = (s32[]{:T(128)}, f32[256,1,2]{0,2,1:T(2,128)S(1)}, f32[256,1,2]{0,2,1:T(2,128)S(1)}, f32[256,1,2,128]{0,3,2,1:T(8,128)S(1)}, s32[16]{0:T(128)S(1)}, ...) while((s32[]{:T(128)}, f32[256,1,2]{0,2,1:T(2,128)S(1)}, ...), condition=%wide.region_5.6_spmd.clone, body=%wide.region_0.5_spmd.clone.sunk | while | flops 103287040 | bytes 4563285 | solution.py:79
  186.6 0.6 dynamic_slice.27
  187.8 4.0 %conditional.3 = ((f32[256,1,2]{0,2,1:T(2,128)S(1)}, f32[256,1,2]{0,2,1:T(2,128)S(1)}, f32[256,1,2,128]{0,3,2,1:T(8,128)S(1)})) conditional(s32[]{:T(128)} %convert_element_type.73, (f32[256,1,2]{0,2,1:T(2,128)S(1)}, f32[256,1,2]{0,2,1:T(2,128)S(1)}, f32[256,1,2,128]{0,3,2,1:T(8,128)S(1)}) %tuple.42, (s32[]{:T(128)}, s32[]{:T(128)}, s32[]{:T(128)}, ...), branch_computations={%region_1.1_spmd, %region_2.4_spmd} | conditional | flops 103287040 | bytes 4562002 | solution.py:75
  190.3 1.3 fusion.4
  191.8 0.6 dynamic_slice.27
  193.1 0.6 dynamic_slice.27
  194.4 0.6 dynamic_slice.27
  195.6 0.6 dynamic_slice.27
  196.9 0.6 dynamic_slice.27
  198.2 0.6 dynamic_slice.27
  199.5 0.6 dynamic_slice.27
  200.7 0.6 dynamic_slice.27
  202.0 0.6 dynamic_slice.27
  203.3 0.6 dynamic_slice.27
  204.5 0.6 dynamic_slice.27
  205.8 0.6 dynamic_slice.27
  207.1 0.6 dynamic_slice.27
  208.3 0.6 dynamic_slice.27
  211.0 0.7 fusion.32
  211.9 39.5 %reduce-scatter.4.cloned.1.call-done = bf16[128,1024]{1,0:T(8,128)(2,1)} async-done(((bf16[2048,1024]{1,0:T(8,128)(2,1)}), bf16[128,1024]{1,0:T(8,128)(2,1)}) %reduce-scatter.4.cloned.1.call-update) | async-done | bytes 262160
  251.4 1.8 reshape.281
  253.3 1.8 copy.59
  255.1 25.9 %all-to-all-start.1 = ((bf16[32,32,128]{2,1,0:T(8,128)(2,1)}), bf16[32,32,128]{2,1,0:T(8,128)(2,1)S(1)}, u32[]{:S(2)}, u32[]{:S(2)}) async-start(bf16[32,32,128]{2,1,0:T(8,128)(2,1)} %copy.59), calls=%async_computation.1 | async-start | bytes 524288 | tf_op jit(solution)/shard_map/all_to_all | solution.py:142
  281.1 32.9 %all-gather.9.cloned.1.call-done = bf16[256,2048]{0,1:T(8,128)(2,1)} async-done(((bf16[256,128]{0,1:T(8,128)(2,1)}), bf16[256,2048]{0,1:T(8,128)(2,1)}) %all-gather.9.cloned.1.call-update) | async-done | bytes 1048592 | tf_op jit(solution)/shard_map/all_gather | solution.py:90
  314.0 2.3 convolution_convert_fusion.1
  316.4 1.3 gather_fusion.1
  317.7 1.1 fusion.29
  (105 shorter events, 4.2 us)
Async XLA Ops:
  7.2 96.6 %copy-start = (bf16[1,256,2048]{2,1,0:T(8,128)(2,1)S(1)}, bf16[1,256,2048]{2,1,0:T(8,128)(2,1)}, u32[]{:S(2)}) copy-start(bf16[1,256,2048]{2,1,0:T(8,128)(2,1)} %param.31) | copy-start | bytes 3145732
  7.2 91.6 %all-gather.11.cloned.1.call-start = ((), (), s32[]{:S(2)}) async-start(), calls=%async_computation.6 | async-start | bytes 4456448 | tf_op jit(solution)/shard_map/all_gather | solution.py:130
  16.5 32.0 %copy-start.3 = (bf16[256,128]{1,0:T(8,128)(2,1)S(1)}, bf16[256,128]{1,0:T(8,128)(2,1)}, u32[]{:S(2)}) copy-start(bf16[256,128]{1,0:T(8,128)(2,1)} %param.19) | copy-start | bytes 196612
  16.5 42.8 %copy-start.4 = (bf16[256,128]{1,0:T(8,128)(2,1)S(1)}, bf16[256,128]{1,0:T(8,128)(2,1)}, u32[]{:S(2)}) copy-start(bf16[256,128]{1,0:T(8,128)(2,1)} %param.20) | copy-start | bytes 196612
  16.5 82.3 %copy-start.9 = (bf16[1,2048,256]{2,1,0:T(8,128)(2,1)S(1)}, bf16[1,2048,256]{2,1,0:T(8,128)(2,1)}, u32[]{:S(2)}) copy-start(bf16[1,2048,256]{2,1,0:T(8,128)(2,1)} %param.29) | copy-start | bytes 3145732
  48.5 106.4 %all-gather.5.cloned.1.call-start = ((), (), s32[]{:S(2)}) async-start(), calls=%async_computation.3 | async-start | bytes 2359296 | tf_op jit(solution)/shard_map/all_gather | solution.py:17
  59.3 43.2 %copy-start.10 = (bf16[1,2048,256]{2,1,0:T(8,128)(2,1)S(1)}, bf16[1,2048,256]{2,1,0:T(8,128)(2,1)}, u32[]{:S(2)}) copy-start(bf16[1,2048,256]{2,1,0:T(8,128)(2,1)} %param.30) | copy-start | bytes 3145732
  59.3 123.3 %all-gather.7.cloned.1.call-start = ((), (), s32[]{:S(2)}) async-start(), calls=%async_computation.4 | async-start | bytes 2359296 | tf_op jit(solution)/shard_map/all_gather | solution.py:17
  70.5 180.9 %reduce-scatter.4.cloned.1.call-start = ((), (), s32[]{:S(2)}) async-start(), calls=%async_computation.7 | async-start | bytes 4456448
  98.8 3.6 %copy-start.8 = (bf16[32,32,2048]{2,1,0:T(8,128)(2,1)S(1)}, bf16[32,32,2048]{2,1,0:T(8,128)(2,1)}, u32[]{:S(2)}) copy-start(bf16[32,32,2048]{2,1,0:T(8,128)(2,1)} %all-gather.11.cloned.1.call-done) | copy-start | bytes 12582916
  153.3 0.8 copy-start.5
  153.3 160.7 %all-gather.9.cloned.1.call-start = ((), (), s32[]{:S(2)}) async-start(), calls=%async_computation.5 | async-start | bytes 1114112 | tf_op jit(solution)/shard_map/all_gather | solution.py:90
  186.5 24.4 %copy-start.7 = (f32[128]{0:T(128)S(1)}, f32[128]{0:T(128)}, u32[]{:S(2)}) copy-start(f32[128]{0:T(128)} %param.22) | copy-start | bytes 1540
  186.6 25.2 %copy-start.2 = (f32[256,8]{0,1:T(8,128)S(1)}, f32[256,8]{0,1:T(8,128)}, u32[]{:S(2)}) copy-start(f32[256,8]{0,1:T(8,128)} %param.27) | copy-start | bytes 24580
  186.6 25.2 %copy-start.6 = (f32[256,2]{0,1:T(2,128)S(1)}, f32[256,2]{0,1:T(2,128)}, u32[]{:S(2)}) copy-start(f32[256,2]{0,1:T(2,128)} %param.28) | copy-start | bytes 6148
  210.9 103.1 %copy-start.1 = (bf16[2048,128]{1,0:T(8,128)(2,1)S(1)}, bf16[2048,128]{1,0:T(8,128)(2,1)}, u32[]{:S(2)}) copy-start(bf16[2048,128]{1,0:T(8,128)(2,1)} %param.23) | copy-start | bytes 1572868
  255.1 61.3 %all-to-all-start.1 = ((bf16[32,32,128]{2,1,0:T(8,128)(2,1)}), bf16[32,32,128]{2,1,0:T(8,128)(2,1)S(1)}, u32[]{:S(2)}, u32[]{:S(2)}) async-start(bf16[32,32,128]{2,1,0:T(8,128)(2,1)} %copy.59), calls=%async_computation.1 | async-start | bytes 524288 | tf_op jit(solution)/shard_map/all_to_all | solution.py:142
Sparse Core Ops, SparseCore 0:
  48.6 50.1 all-gather.10
  100.9 37.4 all-gather.4
  140.5 42.0 all-gather.6
  185.3 66.1 reduce-scatter.3
  254.0 59.9 all-gather.8
where the time goes:
time: 328 us; the launch traced here: 325 us
  waiting for transfers between devices  111 us (34%)
  local copies, waits for them, and re-layouts  94.1 us (29%)
  blocking collectives  46.8 us (14%)
  starting transfers between devices  26.3 us (8%)
  between operations  14.8 us (5%)
  loops' own time  12.6 us (4%)
  matrix products  12.1 us (4%)
  other arithmetic  7.48 us (2%)
    unnamed x30, local copies, waits for them, and re-layouts  64.6 us
    unnamed x6, waiting for transfers between devices  39.6 us
    all_gather x1, waiting for transfers between devices, token_mixer(): lax.all_gather(head_out, 'tp', axis=1, tiled=True)  32.9 us
    all_gather x1, waiting for transfers between devices, expert_block(): experts_arrived = lax.all_gather(arrived, 'tp', axis=2, tiled=True)  28.3 us
    all_to_all x1, starting transfers between devices, expert_block(): lax.all_to_all(answered, EP, split_axis=0, concat_axis=0, tiled=True)  25.9 us
    all_to_all x1, blocking collectives, expert_block(): lax.all_to_all(own_columns, EP, split_axis=0, concat_axis=0, tiled=True)  24.9 us
    all_gather x2, blocking collectives, whole_of(): nearer = lax.all_gather(array, axes[-1], axis=dim, tiled=True)  21.8 us
    another operation x1, loops' own time, token_mixer(): lax.scan(update, state_now, jnp.arange(blocks, dtype=jnp.int32))  10.6 us
  transfers between devices with their start and end apart: 6, of which 4 were waited for; matrix products, arithmetic and copies ran while one was open for 29% of the time, Pallas kernels for 0%

commit v1 on v0

--- a/solution.py
+++ b/solution.py
@@ -87,7 +87,9 @@
         .reshape(row_count, local_heads * value_size)
     )
     mixed = jnp.dot(
-        lax.all_gather(head_out, "tp", axis=1, tiled=True),
+        jnp.concatenate(
+            lax.all_to_all(jnp.stack([head_out] * lax.axis_size("tp")), "tp", 0, 0), axis=1
+        ),
         out_weight,
         preferred_element_type=jnp.float32,
     )

time: 328 us -> 341 us (1.040)
  starting transfers between devices: 26.3 us -> 56.1 us
  waiting for transfers between devices: 111 us -> 94.2 us
    all_gather x1 -> x0, waiting for transfers between devices: 32.9 us -> none  [token_mixer(): lax.all_gather(head_out, 'tp', axis=1, tiled=True)]
    all_to_all x1, starting transfers between devices: 25.9 us -> 44.5 us  [expert_block(): lax.all_to_all(answered, EP, split_axis=0, concat_axis=0, tiled=True)]
    all_to_all x0 -> x1, starting transfers between devices: none -> 11.2 us  [token_mixer(): lax.all_to_all(jnp.stack([head_out] * lax.axis_size('tp')), 'tp', 0, 0)]
    all_to_all x1, waiting for transfers between devices: 0.01 us -> 10.3 us  [expert_block(): lax.all_to_all(answered, EP, split_axis=0, concat_axis=0, tiled=True)]
    unnamed x6 -> x5, waiting for transfers between devices: 39.6 us -> 45.3 us
    unnamed x30 -> x28, local copies, waits for them, and re-layouts: 64.6 us -> 64.8 us
  transfers between devices with their start and end apart: 6 -> 6, of which waited for: 4 -> 4; matrix products, arithmetic and copies ran while one was open for 29% -> 28% of each run, Pallas kernels for 0% -> 0%
where the time goes in v1:
time: 341 us; the launch traced here: 339 us
  local copies, waits for them, and re-layouts  95.4 us (28%)
  waiting for transfers between devices  94.2 us (28%)
  starting transfers between devices  56.1 us (16%)
  blocking collectives  46.8 us (14%)
  between operations  14.8 us (4%)
  loops' own time  12.6 us (4%)
  matrix products  11.9 us (3%)
  other arithmetic  6.86 us (2%)
    unnamed x28, local copies, waits for them, and re-layouts  64.8 us
    unnamed x5, waiting for transfers between devices  45.3 us
    all_to_all x1, starting transfers between devices, expert_block(): lax.all_to_all(answered, EP, split_axis=0, concat_axis=0, tiled=True)  44.5 us
    all_gather x1, waiting for transfers between devices, expert_block(): experts_arrived = lax.all_gather(arrived, 'tp', axis=2, tiled=True)  28.1 us
    all_to_all x1, blocking collectives, expert_block(): lax.all_to_all(own_columns, EP, split_axis=0, concat_axis=0, tiled=True)  24.9 us
    all_gather x2, blocking collectives, whole_of(): nearer = lax.all_gather(array, axes[-1], axis=dim, tiled=True)  21.8 us
    all_to_all x1, starting transfers between devices, token_mixer(): lax.all_to_all(jnp.stack([head_out] * lax.axis_size('tp')), 'tp', 0, 0)  11.2 us
    another operation x1, loops' own time, token_mixer(): lax.scan(update, state_now, jnp.arange(blocks, dtype=jnp.int32))  10.6 us
  transfers between devices with their start and end apart: 6, of which 4 were waited for; matrix products, arithmetic and copies ran while one was open for 28% of the time, Pallas kernels for 0%

profile of v1, /device:TPU:1, one launch (start us, length us, event | category | flops | bytes accessed | tf_op | source)
XLA Modules:
  0.0 338.6 jit_solution(8997258510130477030)
XLA Ops:
  7.2 0.9 copy.53
  8.4 0.7 and_select_fusion
  9.1 1.2 reduce-window.6
  11.0 2.4 scatter_custom_fusion
  13.5 1.5 fusion.21
  15.0 1.5 fusion.23
  16.6 6.0 %gather_fusion = bf16[1024,2048]{1,0:T(8,128)(2,1)} fusion(bf16[256,2048]{1,0:T(8,128)(2,1)S(1)} %fusion.23, s32[1024]{0:T(1024)S(1)} %fusion.38), kind=kCustom, calls=%fused_computation | custom fusion | bytes 8392704 | tf_op jit(solution)/shard_map/gather | solution.py:125
  22.6 1.0 constant_dynamic-slice_fusion
  23.5 24.9 %all_to_all.15 = bf16[32,32,128]{2,1,0:T(8,128)(2,1)} all-to-all(bf16[32,32,128]{2,1,0:T(8,128)(2,1)S(1)} %constant_dynamic-slice_fusion), channel_id=1, replica_groups=mesh['ep_0'=8,'ep_1'=4,'tp'=16] {'ep_0','ep_1'}, dimensions={0} | all-to-all | bytes 524288 | tf_op jit(solution)/shard_map/all_to_all | solution.py:131
  48.6 10.7 %all_gather.15 = bf16[1024,128]{1,0:T(8,128)(2,1)} all-gather(bf16[256,128]{1,0:T(8,128)(2,1)S(1)} %copy-done.2), channel_id=1, replica_groups=mesh['ep_0'=8,'ep_1'=4,'tp'=16] {'ep_1'}, dimensions={0}, use_global_device_ids=true | all-gather | bytes 327680 | tf_op jit(solution)/shard_map/all_gather | solution.py:17
  59.4 11.1 %all_gather.17 = bf16[1024,128]{1,0:T(8,128)(2,1)} all-gather(bf16[256,128]{1,0:T(8,128)(2,1)S(1)} %copy-done.3), channel_id=1, replica_groups=mesh['ep_0'=8,'ep_1'=4,'tp'=16] {'ep_1'}, dimensions={0}, use_global_device_ids=true | all-gather | bytes 327680 | tf_op jit(solution)/shard_map/all_gather | solution.py:17
  70.7 28.1 %all-gather.8.cloned.1.call-done = bf16[32,32,2048]{2,1,0:T(8,128)(2,1)} async-done(((bf16[32,32,128]{2,1,0:T(8,128)(2,1)}), bf16[32,32,2048]{2,1,0:T(8,128)(2,1)}) %all-gather.8.cloned.1.call-update) | async-done | bytes 4194320 | tf_op jit(solution)/shard_map/all_gather | solution.py:132
  98.8 3.6 %fusion.27 = f32[1024,256]{1,0:T(8,128)S(1)} fusion(bf16[1024,2048]{1,0:T(8,128)(2,1)} %bitcast.111, bf16[1,2048,256]{2,1,0:T(8,128)(2,1)S(1)} %copy-done.8), kind=kOutput, calls=%fused_computation.42 | convolution fusion | flops 1073741824 | bytes 6291456 | tf_op jit(solution)/shard_map/dot_general | solution.py:134
  102.4 1.3 fusion.24
  103.7 3.2 convolution_convert_fusion
  106.9 23.0 %copy.59 = bf16[32,32,2048]{1,0,2:T(8,128)(2,1)} copy(bf16[32,32,2048]{2,1,0:T(8,128)(2,1)} %convolution_convert_fusion) | data formatting | bytes 8388608
  130.0 23.3 %reshape.292 = bf16[2048,1024]{1,0:T(8,128)(2,1)} reshape(bf16[2048,32,32]{2,1,0:T(8,128)(2,1)} %bitcast.96) | data formatting | bytes 8388608
  153.3 0.8 copy-done.4
  154.9 8.2 %reshape.291 = bf16[16,512,1,2,64]{4,3,1,0,2:T(2,128)(2,1)} reshape(bf16[8192,128]{1,0:T(8,128)(2,1)} %all-gather.4.cloned.1.call-done) | data formatting | bytes 4194304 | tf_op jit(solution)/shard_map/reshape | solution.py:42
  163.1 9.1 %copy.49 = bf16[16,512,1,2,64]{1,4,3,2,0:T(8,128)(2,1)S(1)} copy(bf16[16,512,1,2,64]{4,3,1,0,2:T(2,128)(2,1)} %reshape.291) | data formatting | bytes 4194304
  172.2 10.4 %all-gather.6.cloned.1.call-done = bf16[8192,128]{1,0:T(8,128)(2,1)} async-done(((bf16[1024,128]{1,0:T(8,128)(2,1)}), bf16[8192,128]{1,0:T(8,128)(2,1)}) %all-gather.6.cloned.1.call-update) | async-done | bytes 2097168 | tf_op jit(solution)/shard_map/all_gather | solution.py:17
  182.7 3.9 %copy.50 = bf16[16,512,1,128]{1,3,2,0:T(8,128)(2,1)} copy(bf16[16,512,1,128]{3,1,0,2:T(8,128)(2,1)} %bitcast.102) | data formatting | bytes 4194304
  186.7 24.3 %while.15 = (s32[]{:T(128)}, f32[256,1,2]{0,2,1:T(2,128)S(1)}, f32[256,1,2]{0,2,1:T(2,128)S(1)}, f32[256,1,2,128]{0,3,2,1:T(8,128)S(1)}, s32[16]{0:T(128)S(1)}, ...) while((s32[]{:T(128)}, f32[256,1,2]{0,2,1:T(2,128)S(1)}, ...), condition=%wide.region_5.6_spmd.clone, body=%wide.region_0.5_spmd.clone.sunk | while | flops 103287040 | bytes 4563285 | solution.py:79
  187.9 4.0 %conditional.3 = ((f32[256,1,2]{0,2,1:T(2,128)S(1)}, f32[256,1,2]{0,2,1:T(2,128)S(1)}, f32[256,1,2,128]{0,3,2,1:T(8,128)S(1)})) conditional(s32[]{:T(128)} %convert_element_type.74, (f32[256,1,2]{0,2,1:T(2,128)S(1)}, f32[256,1,2]{0,2,1:T(2,128)S(1)}, f32[256,1,2,128]{0,3,2,1:T(8,128)S(1)}) %tuple.42, (s32[]{:T(128)}, s32[]{:T(128)}, s32[]{:T(128)}, ...), branch_computations={%region_1.1_spmd, %region_2.4_spmd} | conditional | flops 103287040 | bytes 4562002 | solution.py:75
  190.3 1.3 fusion.4
  191.9 0.6 dynamic_slice.27
  193.2 0.6 dynamic_slice.27
  194.5 0.6 dynamic_slice.27
  195.7 0.6 dynamic_slice.27
  197.0 0.6 dynamic_slice.27
  198.3 0.6 dynamic_slice.27
  199.5 0.6 dynamic_slice.27
  200.8 0.6 dynamic_slice.27
  202.1 0.6 dynamic_slice.27
  203.3 0.6 dynamic_slice.27
  205.9 0.6 dynamic_slice.27
  207.1 0.6 dynamic_slice.27
  208.4 0.6 dynamic_slice.27
  211.2 1.1 stack.3
  212.2 11.2 %all-to-all-start = ((bf16[16,256,128]{1,2,0:T(8,128)(2,1)}), bf16[16,256,128]{1,2,0:T(8,128)(2,1)S(1)}, u32[]{:S(2)}, u32[]{:S(2)}) async-start(bf16[16,256,128]{1,2,0:T(8,128)(2,1)} %stack.3), calls=%async_computation | async-start | bytes 2097152 | tf_op jit(solution)/shard_map/all_to_all | solution.py:91
  223.6 45.2 %reduce-scatter.4.cloned.1.call-done = bf16[128,1024]{1,0:T(8,128)(2,1)} async-done(((bf16[2048,1024]{1,0:T(8,128)(2,1)}), bf16[128,1024]{1,0:T(8,128)(2,1)}) %reduce-scatter.4.cloned.1.call-update) | async-done | bytes 262160
  268.8 1.8 reshape.293
  270.7 1.8 copy.60
  272.5 44.5 %all-to-all-start.2 = ((bf16[32,32,128]{2,1,0:T(8,128)(2,1)}), bf16[32,32,128]{2,1,0:T(8,128)(2,1)S(1)}, u32[]{:S(2)}, u32[]{:S(2)}) async-start(bf16[32,32,128]{2,1,0:T(8,128)(2,1)} %copy.60), calls=%async_computation.2 | async-start | bytes 524288 | tf_op jit(solution)/shard_map/all_to_all | solution.py:144
  317.2 2.2 convolution_convert_fusion.1
  319.3 10.3 %all-to-all-done.2 = bf16[32,32,128]{2,1,0:T(8,128)(2,1)S(1)} async-done(((bf16[32,32,128]{2,1,0:T(8,128)(2,1)}), bf16[32,32,128]{2,1,0:T(8,128)(2,1)S(1)}, u32[]{:S(2)}, u32[]{:S(2)}) %all-to-all-start.2) | async-done | bytes 262176 | tf_op jit(solution)/shard_map/all_to_all | solution.py:144
  329.6 1.3 gather_fusion.1
  331.0 1.1 fusion.29
  (103 shorter events, 4.8 us)
Async XLA Ops:
  7.2 96.6 %copy-start = (bf16[1,256,2048]{2,1,0:T(8,128)(2,1)S(1)}, bf16[1,256,2048]{2,1,0:T(8,128)(2,1)}, u32[]{:S(2)}) copy-start(bf16[1,256,2048]{2,1,0:T(8,128)(2,1)} %param.31) | copy-start | bytes 3145732
  7.2 91.6 %all-gather.8.cloned.1.call-start = ((), (), s32[]{:S(2)}) async-start(), calls=%async_computation.6 | async-start | bytes 4456448 | tf_op jit(solution)/shard_map/all_gather | solution.py:132
  16.5 32.0 %copy-start.2 = (bf16[256,128]{1,0:T(8,128)(2,1)S(1)}, bf16[256,128]{1,0:T(8,128)(2,1)}, u32[]{:S(2)}) copy-start(bf16[256,128]{1,0:T(8,128)(2,1)} %param.19) | copy-start | bytes 196612
  16.5 42.8 %copy-start.3 = (bf16[256,128]{1,0:T(8,128)(2,1)S(1)}, bf16[256,128]{1,0:T(8,128)(2,1)}, u32[]{:S(2)}) copy-start(bf16[256,128]{1,0:T(8,128)(2,1)} %param.20) | copy-start | bytes 196612
  16.5 82.3 %copy-start.8 = (bf16[1,2048,256]{2,1,0:T(8,128)(2,1)S(1)}, bf16[1,2048,256]{2,1,0:T(8,128)(2,1)}, u32[]{:S(2)}) copy-start(bf16[1,2048,256]{2,1,0:T(8,128)(2,1)} %param.29) | copy-start | bytes 3145732
  48.5 106.4 %all-gather.4.cloned.1.call-start = ((), (), s32[]{:S(2)}) async-start(), calls=%async_computation.4 | async-start | bytes 2359296 | tf_op jit(solution)/shard_map/all_gather | solution.py:17
  59.3 43.2 %copy-start.9 = (bf16[1,2048,256]{2,1,0:T(8,128)(2,1)S(1)}, bf16[1,2048,256]{2,1,0:T(8,128)(2,1)}, u32[]{:S(2)}) copy-start(bf16[1,2048,256]{2,1,0:T(8,128)(2,1)} %param.30) | copy-start | bytes 3145732
  59.3 123.4 %all-gather.6.cloned.1.call-start = ((), (), s32[]{:S(2)}) async-start(), calls=%async_computation.5 | async-start | bytes 2359296 | tf_op jit(solution)/shard_map/all_gather | solution.py:17
  70.5 198.3 %reduce-scatter.4.cloned.1.call-start = ((), (), s32[]{:S(2)}) async-start(), calls=%async_computation.7 | async-start | bytes 4456448
  98.8 3.6 %copy-start.7 = (bf16[32,32,2048]{2,1,0:T(8,128)(2,1)S(1)}, bf16[32,32,2048]{2,1,0:T(8,128)(2,1)}, u32[]{:S(2)}) copy-start(bf16[32,32,2048]{2,1,0:T(8,128)(2,1)} %all-gather.8.cloned.1.call-done) | copy-start | bytes 12582916
  153.3 0.8 copy-start.4
  186.7 24.4 %copy-start.6 = (f32[128]{0:T(128)S(1)}, f32[128]{0:T(128)}, u32[]{:S(2)}) copy-start(f32[128]{0:T(128)} %param.22) | copy-start | bytes 1540
  210.9 12.5 %copy-start.1 = (f32[256,8]{0,1:T(8,128)S(1)}, f32[256,8]{0,1:T(8,128)}, u32[]{:S(2)}) copy-start(f32[256,8]{0,1:T(8,128)} %param.27) | copy-start | bytes 24580
  210.9 12.5 %copy-start.5 = (f32[256,2]{0,1:T(2,128)S(1)}, f32[256,2]{0,1:T(2,128)}, u32[]{:S(2)}) copy-start(f32[256,2]{0,1:T(2,128)} %param.28) | copy-start | bytes 6148
  212.2 60.2 %all-to-all-start = ((bf16[16,256,128]{1,2,0:T(8,128)(2,1)}), bf16[16,256,128]{1,2,0:T(8,128)(2,1)S(1)}, u32[]{:S(2)}, u32[]{:S(2)}) async-start(bf16[16,256,128]{1,2,0:T(8,128)(2,1)} %stack.3), calls=%async_computation | async-start | bytes 2097152 | tf_op jit(solution)/shard_map/all_to_all | solution.py:91
  272.5 57.2 %all-to-all-start.2 = ((bf16[32,32,128]{2,1,0:T(8,128)(2,1)}), bf16[32,32,128]{2,1,0:T(8,128)(2,1)S(1)}, u32[]{:S(2)}, u32[]{:S(2)}) async-start(bf16[32,32,128]{2,1,0:T(8,128)(2,1)} %copy.60), calls=%async_computation.2 | async-start | bytes 524288 | tf_op jit(solution)/shard_map/all_to_all | solution.py:144
Sparse Core Ops, SparseCore 0:
  48.6 50.1 all-gather.7
  100.9 37.2 all-gather.3
  140.3 42.3 all-gather.5
  185.4 83.3 reduce-scatter.3
